TPU v7x, 32 devices: a whole 2x2x4 slice. The times are simulated.
32 devices in a mesh: ep: 32 (over z, y, x, core).
Axes of the slice: x: 2, y: 2, z: 4, core: 2. Of those that a mesh axis runs over, the one named last changes fastest.
Arguments:
- residual_in: bfloat16 [256, 2048], P('ep'), may hold values from -6 to 6
- gain_mix_pre: float32 [2048], replicated, may hold values from 0.1 to 1.9
- w_query: bfloat16 [2048, 2048], P(None, 'ep'), may hold values from -0.125 to 0.125
- w_key: bfloat16 [2048, 2048], P(None, 'ep'), may hold values from -0.125 to 0.125
- w_value: bfloat16 [2048, 2048], P(None, 'ep'), may hold values from -0.125 to 0.125
- w_outgate: bfloat16 [2048, 2048], P(None, 'ep'), may hold values from -0.125 to 0.125
- w_decay: bfloat16 [2048, 16], replicated, may hold values from -0.125 to 0.125
- w_beta: bfloat16 [2048, 16], replicated, may hold values from -0.125 to 0.125
- decay_scale: float32 [16], replicated, may hold values from 1 to 16
- decay_bias: float32 [16], replicated, may hold values from -5 to -1
- head_gain: float32 [128], replicated, may hold values from 0.1 to 1.9
- w_out: bfloat16 [2048, 2048], replicated, may hold values from -0.125 to 0.125
- gain_mix_post: float32 [2048], replicated, may hold values from 0.1 to 1.9
- state_cache: bfloat16 [256, 16, 128, 128], P('ep'), may hold values from -2.390625 to 2.390625
- gain_ffn_pre: float32 [2048], replicated, may hold values from 0.1 to 1.9
- routes: int32 [256, 4], P('ep'), may hold values from 0 to 7, all different within a row; in each aligned block of 8 rows (0 to 7, 8 to 15, ...) at most 8 rows name the same one
- route_logits: float32 [256, 4], P('ep'), may hold values from -6 to 6
- w_gate: bfloat16 [2048, 16384], P(None, 'ep'), may hold values from -0.375 to 0.375
- w_up: bfloat16 [2048, 16384], P(None, 'ep'), may hold values from -0.375 to 0.375
- w_down: bfloat16 [16384, 2048], P('ep'), may hold values from -0.125 to 0.125
- gain_ffn_post: float32 [2048], replicated, may hold values from 0.1 to 1.9
Outputs:
- result: bfloat16 [256, 2048], P('ep')
- new_state: bfloat16 [256, 16, 128, 128], P('ep')
Inputs may be any that keep to these rules, and one draw needn't show every extreme that they name: `routes`: each row names 4 different experts. In the rows of one device (aligned blocks of 8 rows) no expert is named more than 8 times, and in some block one expert is named exactly 8 times.
All inputs are finite; a program needn't handle non-finite values.
Results may differ from a plain program's by a relative error of at most 0.014.
Values may be sent and summed in bfloat16 or wider, within the bound.
A program may use at most 128 MiB of HBM per device.

v0:
```python
import functools

import jax
import jax.numpy as jnp
from jax import lax
from jax.experimental import pallas as pl
from jax.experimental.pallas import tpu as pltpu
from jax.sharding import PartitionSpec as P

H = 16
HD = 128
PIECES = 4
TOPK = 4
LANES = 128
TAIL = 2 * LANES
VMEM_LIMIT = 66 * 1000 * 1000
MESH = pl.DeviceIdType.MESH

EPS = 1e-06
LIMIT = 7.0
ALPHA = 1.702


def rms_scale(values):
    return values * lax.rsqrt(jnp.mean(values * values, axis=-1, keepdims=True) + EPS)


def clamped_unit(gate, upper):
    glu = jnp.minimum(gate, LIMIT)
    linear = jnp.clip(upper, -LIMIT, LIMIT)
    return glu * jax.nn.sigmoid(ALPHA * glu) * (linear + 1.0)


def flipped(value, distance):
    bit = 1
    while bit <= distance:
        if distance & bit:
            value = value + bit - 2 * bit * (lax.rem(value // bit, 2))
        bit *= 2
    return value


class Place:
    def __init__(self, devices):
        self.devices = devices
        self.layers = devices // 8
        self.me = lax.axis_index("ep")
        self.core = lax.rem(self.me, 2)
        self.x = lax.rem(self.me // 2, 2)
        self.y = lax.rem(self.me // 4, 2)
        self.z = self.me // 8

    def at(self, distance=0, y=0, x=0, core=0):
        z = flipped(self.z, distance)
        return (
            z * 8
            + flipped(self.y, y) * 4
            + flipped(self.x, x) * 2
            + flipped(self.core, core)
        )

    def partners(self):
        return [self.at(d) for d in range(1, self.layers)] + [
            self.at(y=1),
            self.at(x=1),
            self.at(core=1),
        ]


def greet(partners):
    barrier = pltpu.get_barrier_semaphore()
    for partner in partners:
        pl.semaphore_signal(barrier, inc=1, device_id=(partner,), device_id_type=MESH)
    return lambda: pl.semaphore_wait(barrier, len(partners))


def load_all(pairs, sems):
    loads = [
        pltpu.make_async_copy(source, target, sems.at[i])
        for i, (source, target) in enumerate(pairs)
    ]
    for load in loads:
        load.start()
    return loads


def remote(source, target, send_sem, recv_sem, device):
    return pltpu.make_async_remote_copy(
        src_ref=source,
        dst_ref=target,
        send_sem=send_sem,
        recv_sem=recv_sem,
        device_id=(device,),
        device_id_type=MESH,
    )


def gather_sends(devices):
    layers = devices // 8
    return layers - 1 + 3 * layers + devices // 2


def gather_blocks(place, buf, send_sems, recv_sems):
    started = []

    def push(block, device):
        copy = remote(
            buf.at[block], buf.at[block], send_sems.at[len(started)], recv_sems.at[block], device
        )
        copy.start()
        started.append(copy)

    def arrive(block):
        remote(
            buf.at[block], buf.at[block], send_sems.at[0], recv_sems.at[block], place.at(core=1)
        ).wait_recv()

    def spread(distance):
        block = place.at(distance)
        push(block, place.at(x=1))
        push(block, place.at(y=1))
        push(block, place.at(core=1))

    def onward(distance):
        across_x, across_y = place.at(distance, x=1), place.at(distance, y=1)
        arrive(across_x)
        if distance % 2 == 0:
            push(across_x, place.at(y=1))
        push(across_x, place.at(core=1))
        arrive(across_y)
        if distance % 2 == 1:
            push(across_y, place.at(x=1))
        push(across_y, place.at(core=1))

    layers = place.layers
    for distance in range(layers - 1, 0, -1):
        push(place.me, place.at(distance))
    spread(0)
    for distance in range(1, layers):
        arrive(place.at(distance))
        spread(distance)
        onward(distance - 1)
    onward(layers - 1)
    for distance in range(layers):
        diagonal = place.at(distance, y=1, x=1)
        arrive(diagonal)
        push(diagonal, place.at(core=1))
    for distance in range(layers):
        for y in range(2):
            for x in range(2):
                arrive(place.at(distance, y, x, 1))
    return started


def settle(started):
    for copy in started:
        copy.wait_send()


def reduce_blocks(place, mine, paired, total, second, third, fourth, sems):
    pair_recv, send_sems, second_recv, third_recv, fourth_recv = sems
    started = []
    layers = place.layers

    def push(source, target, recv_sem, device):
        copy = remote(source, target, send_sems.at[len(started)], recv_sem, device)
        copy.start()
        started.append(copy)

    def arrive(target, recv_sem):
        remote(target, target, send_sems.at[0], recv_sem, place.at(core=1)).wait_recv()

    def wide(block):
        return block.astype(jnp.float32)

    order = list(range(layers - 1, -1, -1))
    for distance in order:
        for y, x in ((1, 1), (0, 1), (1, 0), (0, 0)):
            k = place.at(distance, y, x) // 2
            arrive(paired.at[k], pair_recv.at[k])
            total[k] = (wide(mine[k]) + wide(paired[k])).astype(jnp.bfloat16)
    for distance in order:
        if distance % 2 == 0:
            first, far, near = place.at(y=1), (1, 1), (1, 0)
        else:
            first, far, near = place.at(x=1), (1, 1), (0, 1)
        for slot, (y, x) in ((1, far), (0, near)):
            k = place.at(distance, y, x) // 2
            at = 2 * distance + slot
            push(total.at[k], second.at[at], second_recv.at[at], first)
    for distance in order:
        if distance % 2 == 0:
            then, (y, x) = place.at(x=1), (0, 1)
        else:
            then, (y, x) = place.at(y=1), (1, 0)
        k = place.at(distance, y, x) // 2
        at = 2 * distance + 1
        arrive(second.at[at], second_recv.at[at])
        total[k] = (wide(total[k]) + wide(second[at])).astype(jnp.bfloat16)
        push(total.at[k], third.at[distance], third_recv.at[distance], then)
    for distance in order:
        k = place.at(distance) // 2
        at = 2 * distance
        arrive(second.at[at], second_recv.at[at])
        arrive(third.at[distance], third_recv.at[distance])
        value = wide(total[k]) + wide(second[at]) + wide(third[distance])
        if distance > 0:
            total[k] = value.astype(jnp.bfloat16)
            push(total.at[k], fourth.at[distance], fourth_recv.at[distance], place.at(distance))
    for distance in range(1, layers):
        arrive(fourth.at[distance], fourth_recv.at[distance])
        value = value + wide(fourth[distance])
    return value, started


def dot_t(left, right):
    return lax.dot_general(
        left, right, (((1,), (1,)), ((), ())), preferred_element_type=jnp.float32
    )


def column_of(row):
    size = row.shape[1]
    across = lax.broadcasted_iota(jnp.int32, (size, size), 1)
    down = lax.broadcasted_iota(jnp.int32, (size, size), 0)
    return jnp.sum(
        jnp.where(across == down, jnp.broadcast_to(row, (size, size)), 0.0), axis=1, keepdims=True
    )


def project_kernel(
    devices,
    own,
    x_hbm,
    gain_hbm,
    routes_hbm,
    logits_hbm,
    decay_hbm,
    beta_hbm,
    q_hbm,
    k_hbm,
    v_hbm,
    z_hbm,
    joined,
    shares_ref,
    decay_out,
    beta_out,
    x_ref,
    gain_ref,
    routes_ref,
    logits_ref,
    decay_ref,
    beta_ref,
    weights,
    buf,
    columns,
    send_sems,
    recv_sems,
    out_sems,
    in_sems,
    load_sems,
):
    place = Place(devices)
    others = [lax.rem(place.me + i, devices) for i in range(1, devices)]
    ready = greet(others)
    count, width = x_ref.shape
    loads = load_all(
        [
            (x_hbm, x_ref),
            (gain_hbm, gain_ref),
            (routes_hbm, routes_ref),
            (logits_hbm, logits_ref),
            (decay_hbm, decay_ref),
            (beta_hbm, beta_ref),
        ]
        + [
            (ref, weights.at[pl.ds(i * own, own)])
            for i, ref in enumerate((q_hbm, k_hbm, v_hbm, z_hbm))
        ],
        load_sems,
    )
    for load in loads[:4]:
        load.wait()
    normed = (rms_scale(x_ref[...].astype(jnp.float32)) * gain_ref[...]).astype(jnp.bfloat16)
    raised = jnp.exp(logits_ref[...])
    shares = raised / jnp.sum(raised, axis=0, keepdims=True)
    routes = routes_ref[...].astype(jnp.float32)
    lane = lax.broadcasted_iota(jnp.int32, (count, LANES), 1).astype(jnp.float32)
    share = jnp.zeros(lane.shape, jnp.float32)
    for j in range(routes.shape[0]):
        share = share + jnp.where(
            lane == column_of(routes[j : j + 1]), column_of(shares[j : j + 1]), 0.0
        )
    high = share.astype(jnp.bfloat16)
    low = (share - high.astype(jnp.float32)).astype(jnp.bfloat16)
    buf[place.me, :, 0:width] = normed
    buf[place.me, :, width : width + LANES] = high
    buf[place.me, :, width + LANES : width + TAIL] = low
    ready()
    started = gather_blocks(place, buf, send_sems, recv_sems)
    for load in loads[4:]:
        load.wait()
    rows = buf[:, :, 0:width].reshape(devices * count, width)
    columns[...] = dot_t(rows, weights[...]).astype(jnp.bfloat16).reshape(columns.shape)
    for i, other in enumerate(others):
        copy = remote(
            columns.at[other], joined.at[place.me], out_sems.at[i], in_sems.at[place.me], other
        )
        copy.start()
        started.append(copy)
    joined[place.me] = columns[place.me]
    decay_out[...] = dot_t(normed, decay_ref[...])
    beta_out[...] = dot_t(normed, beta_ref[...])
    shares_ref[...] = buf[:, :, width:]
    for other in others:
        remote(
            columns.at[other], joined.at[other], out_sems.at[0], in_sems.at[other], other
        ).wait_recv()
    settle(started)


def project(devices, x, gain, routes, logits, w_query, w_key, w_value, w_outgate, w_decay, w_beta):
    count, width = x.shape
    own = w_query.shape[1]
    block = max(4 * own, LANES)
    vmem = pl.BlockSpec(memory_space=pltpu.VMEM)
    hbm = pl.BlockSpec(memory_space=pltpu.HBM)
    heads = w_decay.shape[1]
    dma = pltpu.SemaphoreType.DMA
    inputs = (
        x,
        gain[None],
        routes.T,
        logits.T,
        w_decay.T,
        w_beta.T,
        w_query.T,
        w_key.T,
        w_value.T,
        w_outgate.T,
    )
    return pl.pallas_call(
        functools.partial(project_kernel, devices, own),
        out_shape=(
            jax.ShapeDtypeStruct((devices, count, block), jnp.bfloat16),
            jax.ShapeDtypeStruct((devices, count, TAIL), jnp.bfloat16),
            jax.ShapeDtypeStruct((count, heads), jnp.float32),
            jax.ShapeDtypeStruct((count, heads), jnp.float32),
        ),
        in_specs=[hbm] * len(inputs),
        out_specs=(vmem,) * 4,
        scratch_shapes=[pltpu.VMEM(a.shape, a.dtype) for a in inputs[:6]]
        + [
            pltpu.VMEM((block, width), jnp.bfloat16),
            pltpu.VMEM((devices, count, width + TAIL), jnp.bfloat16),
            pltpu.VMEM((devices, count, block), jnp.bfloat16),
            dma((gather_sends(devices),)),
            dma((devices,)),
            dma((devices,)),
            dma((devices,)),
            dma((len(inputs),)),
        ],
        compiler_params=pltpu.CompilerParams(
            collective_id=0, has_side_effects=True, vmem_limit_bytes=VMEM_LIMIT
        ),
    )(*inputs)


def head_rows(joined, head, kind, own):
    lane = lax.broadcasted_iota(jnp.int32, (joined.shape[1], LANES), 1)
    value = jnp.zeros(lane.shape, jnp.float32)
    group, offset = divmod(kind * own, LANES)
    for i in range(HD // own):
        piece = joined[head * (HD // own) + i, :, group * LANES : (group + 1) * LANES]
        piece = piece.astype(jnp.float32)
        shift = (i * own - offset) % LANES
        if shift:
            piece = pltpu.roll(piece, shift, 1)
        value = jnp.where((lane >= i * own) & (lane < (i + 1) * own), piece, value)
    return value


def delta_kernel(
    own,
    joined,
    decay_in,
    beta_in,
    scale_ref,
    bias_ref,
    head_gain_ref,
    state_hbm,
    w_out_hbm,
    branch_ref,
    new_hbm,
    state,
    fresh,
    w_out,
    mixed,
    state_sems,
    fresh_sems,
    out_sems,
):
    heads = mixed.shape[0]
    count = state.shape[0]
    width = w_out.shape[1]

    def state_in(h):
        return pltpu.make_async_copy(state_hbm.at[:, h], state.at[:, h], state_sems.at[h])

    def state_out(h):
        return pltpu.make_async_copy(fresh.at[:, h], new_hbm.at[:, h], fresh_sems.at[h])

    for h in range(heads):
        state_in(h).start()
    w_load = pltpu.make_async_copy(w_out_hbm, w_out, out_sems.at[0])
    w_load.start()
    decay = jnp.exp(-scale_ref[...] * jax.nn.softplus(decay_in[...] + bias_ref[...]))
    strength = jax.nn.sigmoid(beta_in[...])
    lane = lax.broadcasted_iota(jnp.int32, decay.shape, 1)

    def one(h, carry):
        query = jax.nn.silu(head_rows(joined, h, 0, own))
        query = (
            query * lax.rsqrt(jnp.sum(query * query, axis=-1, keepdims=True) + EPS) * HD ** (-0.5)
        )
        keys = jax.nn.silu(head_rows(joined, h, 1, own))
        keys = keys * lax.rsqrt(jnp.sum(keys * keys, axis=-1, keepdims=True) + EPS)
        values = jax.nn.silu(head_rows(joined, h, 2, own))
        outgate = jax.nn.silu(head_rows(joined, h, 3, own))
        keep = jnp.sum(jnp.where(lane == h, decay, 0.0), axis=1, keepdims=True)
        beta = jnp.sum(jnp.where(lane == h, strength, 0.0), axis=1, keepdims=True)
        overlap = jnp.sum(keys * query, axis=1, keepdims=True)
        upright = jnp.transpose(jnp.concatenate([keys, query], axis=0))
        state_in(h).wait()
        outputs = []
        for r in range(count):
            held = state[r, h].astype(jnp.float32)
            key = jnp.broadcast_to(upright[:, r : r + 1], held.shape)
            ask = jnp.broadcast_to(upright[:, count + r : count + r + 1], held.shape)
            rate = keep[r : r + 1]
            guess = rate * jnp.sum(key * held, axis=0, keepdims=True)
            change = beta[r : r + 1] * (values[r : r + 1] - guess)
            seen = rate * jnp.sum(ask * held, axis=0, keepdims=True)
            outputs.append(seen + overlap[r : r + 1] * change)
            fresh[r, h] = (rate * held + key * change).astype(jnp.bfloat16)
        state_out(h).start()
        output = rms_scale(jnp.concatenate(outputs, axis=0)) * head_gain_ref[...]
        mixed[h] = (output * outgate).astype(jnp.bfloat16)
        return carry

    lax.fori_loop(0, heads, one, 0)
    w_load.wait()
    rows = jnp.concatenate([mixed[h] for h in range(heads)], axis=1)
    for j in range(0, width, 512):
        branch_ref[:, j : j + 512] = jnp.dot(
            rows, w_out[:, j : j + 512], preferred_element_type=jnp.float32
        )
    for h in range(heads):
        state_out(h).wait()


def delta_part(own, joined, decay_in, beta_in, scale, bias, head_gain, state, w_out):
    count, heads = state.shape[:2]
    vmem = pl.BlockSpec(memory_space=pltpu.VMEM)
    hbm = pl.BlockSpec(memory_space=pltpu.HBM)
    dma = pltpu.SemaphoreType.DMA
    return pl.pallas_call(
        functools.partial(delta_kernel, own),
        out_shape=(
            jax.ShapeDtypeStruct((count, w_out.shape[1]), jnp.float32),
            jax.ShapeDtypeStruct(state.shape, state.dtype),
        ),
        in_specs=[vmem] * 6 + [hbm] * 2,
        out_specs=(vmem, hbm),
        scratch_shapes=[
            pltpu.VMEM(state.shape, state.dtype),
            pltpu.VMEM(state.shape, state.dtype),
            pltpu.VMEM(w_out.shape, w_out.dtype),
            pltpu.VMEM((heads, count, HD), jnp.bfloat16),
            dma((heads,)),
            dma((heads,)),
            dma((1,)),
        ],
        compiler_params=pltpu.CompilerParams(vmem_limit_bytes=VMEM_LIMIT),
    )(joined, decay_in, beta_in, scale[None], bias[None], head_gain[None], state, w_out)


def expert_kernel(
    devices,
    branch_ref,
    shares_ref,
    x_hbm,
    gain_mix_hbm,
    gain_pre_hbm,
    gain_post_hbm,
    gate_hbm,
    up_hbm,
    down_hbm,
    result_ref,
    x_ref,
    gain_mix_ref,
    gain_pre_ref,
    gain_post_ref,
    small_sems,
    buf,
    gate,
    up,
    down,
    hidden,
    weight,
    theirs,
    mine,
    paired,
    total,
    second,
    third,
    fourth,
    gather_send,
    gather_recv,
    load_sems,
    pair_send,
    pair_recv,
    sum_send,
    second_recv,
    third_recv,
    fourth_recv,
):
    place = Place(devices)
    ready = greet(place.partners())
    small = load_all(
        [
            (x_hbm, x_ref),
            (gain_mix_hbm, gain_mix_ref),
            (gain_pre_hbm, gain_pre_ref),
            (gain_post_hbm, gain_post_ref),
        ],
        small_sems,
    )
    loads = load_all([(gate_hbm, gate), (up_hbm, up), (down_hbm, down)], load_sems)
    for load in small:
        load.wait()
    count, width = x_ref.shape
    pieces = gate.shape[1]
    pairs = devices // 2
    x_second = x_ref[...].astype(jnp.float32) + rms_scale(branch_ref[...]) * gain_mix_ref[...]
    buf[place.me] = (rms_scale(x_second) * gain_pre_ref[...]).astype(jnp.bfloat16)
    ready()
    started = gather_blocks(place, buf, gather_send, gather_recv)
    share = shares_ref[:, :, 0:LANES].astype(jnp.float32) + shares_ref[:, :, LANES:].astype(
        jnp.float32
    )
    share = share.reshape(devices * count, LANES)
    lane = lax.broadcasted_iota(jnp.int32, share.shape, 1)
    share = jnp.sum(jnp.where(lane == place.me // PIECES, share, 0.0), axis=1, keepdims=True)
    weight[...] = jnp.broadcast_to(share, (devices * count, LANES)).reshape(weight.shape)
    loads[0].wait()
    loads[1].wait()
    rows = buf[...].reshape(devices * count, width)
    step = 256
    for j in range(0, pieces, step):
        gated = clamped_unit(
            jnp.dot(rows, gate[:, j : j + step], preferred_element_type=jnp.float32),
            jnp.dot(rows, up[:, j : j + step], preferred_element_type=jnp.float32),
        )
        hidden[:, :, :, j : j + step] = gated.astype(jnp.bfloat16).reshape(
            pairs, 2, count, step
        )
    loads[2].wait()

    def parts(core, out):
        units = hidden[:, core].reshape(pairs * count, pieces)
        scale = weight[:, core].reshape(pairs * count, LANES)[:, 0:1]
        for j in range(0, width, 512):
            part = jnp.dot(units, down[:, j : j + 512], preferred_element_type=jnp.float32)
            out[:, :, j : j + 512] = (
                (part * scale).astype(jnp.bfloat16).reshape(pairs, count, 512)
            )

    parts(1 - place.core, theirs)
    sent = []
    for distance in range(place.layers - 1, -1, -1):
        for y, x in ((1, 1), (0, 1), (1, 0), (0, 0)):
            k = place.at(distance, y, x) // 2
            copy = remote(
                theirs.at[k],
                paired.at[k],
                pair_send.at[len(sent)],
                pair_recv.at[k],
                place.at(core=1),
            )
            copy.start()
            sent.append(copy)
    parts(place.core, mine)
    moe, more = reduce_blocks(
        place,
        mine,
        paired,
        total,
        second,
        third,
        fourth,
        (pair_recv, sum_send, second_recv, third_recv, fourth_recv),
    )
    result_ref[...] = (x_second + rms_scale(moe) * gain_post_ref[...]).astype(jnp.bfloat16)
    settle(started + sent + more)


def experts_part(
    devices, branch, x, gain_mix, gain_pre, gain_post, shares, w_gate, w_up, w_down
):
    count, width = x.shape
    layers = devices // 8
    pairs = devices // 2
    pieces = w_gate.shape[1]
    vmem = pl.BlockSpec(memory_space=pltpu.VMEM)
    hbm = pl.BlockSpec(memory_space=pltpu.HBM)
    dma = pltpu.SemaphoreType.DMA

    def blocks(number):
        return pltpu.VMEM((number, count, width), jnp.bfloat16)

    return pl.pallas_call(
        functools.partial(expert_kernel, devices),
        out_shape=jax.ShapeDtypeStruct((count, width), jnp.bfloat16),
        in_specs=[vmem] * 2 + [hbm] * 7,
        out_specs=vmem,
        scratch_shapes=[
            pltpu.VMEM(x.shape, x.dtype),
            pltpu.VMEM((1, width), jnp.float32),
            pltpu.VMEM((1, width), jnp.float32),
            pltpu.VMEM((1, width), jnp.float32),
            dma((4,)),
            blocks(devices),
            pltpu.VMEM(w_gate.shape, jnp.bfloat16),
            pltpu.VMEM(w_up.shape, jnp.bfloat16),
            pltpu.VMEM(w_down.shape, jnp.bfloat16),
            pltpu.VMEM((pairs, 2, count, pieces), jnp.bfloat16),
            pltpu.VMEM((pairs, 2, count, LANES), jnp.float32),
            blocks(pairs),
            blocks(pairs),
            blocks(pairs),
            blocks(pairs),
            blocks(2 * layers),
            blocks(layers),
            blocks(layers),
            dma((gather_sends(devices),)),
            dma((devices,)),
            dma((3,)),
            dma((pairs,)),
            dma((pairs,)),
            dma((4 * layers,)),
            dma((2 * layers,)),
            dma((layers,)),
            dma((layers,)),
        ],
        compiler_params=pltpu.CompilerParams(
            collective_id=1, has_side_effects=True, vmem_limit_bytes=VMEM_LIMIT
        ),
    )(
        branch,
        shares,
        x,
        gain_mix[None],
        gain_pre[None],
        gain_post[None],
        w_gate,
        w_up,
        w_down,
    )


def shards(
    residual_in,
    gain_mix_pre,
    w_query,
    w_key,
    w_value,
    w_outgate,
    w_decay,
    w_beta,
    decay_scale,
    decay_bias,
    head_gain,
    w_out,
    gain_mix_post,
    state_cache,
    gain_ffn_pre,
    routes,
    route_logits,
    w_gate,
    w_up,
    w_down,
    gain_ffn_post,
):
    devices = lax.axis_size("ep")
    joined, shares, decay_in, beta_in = project(
        devices,
        residual_in,
        gain_mix_pre,
        routes,
        route_logits,
        w_query,
        w_key,
        w_value,
        w_outgate,
        w_decay,
        w_beta,
    )
    branch, new_state = delta_part(
        w_query.shape[1],
        joined,
        decay_in,
        beta_in,
        decay_scale,
        decay_bias,
        head_gain,
        state_cache,
        w_out,
    )
    result = experts_part(
        devices,
        branch,
        residual_in,
        gain_mix_post,
        gain_ffn_pre,
        gain_ffn_post,
        shares,
        w_gate,
        w_up,
        w_down,
    )
    return (result, new_state)


def solution(mesh):
    in_specs = (
        P("ep", None),
        P(),
        P(None, "ep"),
        P(None, "ep"),
        P(None, "ep"),
        P(None, "ep"),
        P(),
        P(),
        P(),
        P(),
        P(),
        P(),
        P(),
        P("ep", None, None, None),
        P(),
        P("ep", None),
        P("ep", None),
        P(None, "ep"),
        P(None, "ep"),
        P("ep", None),
        P(),
    )
    out_specs = (P("ep", None), P("ep", None, None, None))
    return jax.shard_map(shards, mesh=mesh, in_specs=in_specs, out_specs=out_specs, check_vma=False)
```

profile of v0, /device:TPU:0, one launch (start us, length us, event | category | flops | bytes accessed | tf_op | source)
XLA Modules:
  0.0 81.3 jit_solution(17663811210815289761)
XLA Ops:
  0.6 27.3 %shard_map.212 = (bf16[32,8,256]{2,1,0:T(8,128)(2,1)}, bf16[32,8,256]{2,1,0:T(8,128)(2,1)}, f32[8,16]{1,0:T(8,128)}, f32[8,16]{1,0:T(8,128)}) custom-call(bf16[8,2048]{1,0:T(8,128)(2,1)} %x_hbm.3, f32[1,2048]{1,0:T(1,128)} %bitcast.21, s32[4,8]{1,0:T(4,128)} %bitcast.25, f32[4,8]{1,0:T(4,128)} %bitcast.26, bf16[16,2048]{1,0:T(8,128)(2,1)} %bitcast.19, ...), custom_call_target="tpu_custom_call" | custom-call | tf_op jit(solution)/shard_map/pallas_call | solution.py:342
  28.0 16.3 %shard_map.213 = (f32[8,2048]{1,0:T(8,128)}, bf16[8,16,128,128]{3,2,1,0:T(8,128)(2,1)}) custom-call(bf16[32,8,256]{2,1,0:T(8,128)(2,1)} %get-tuple-element.8.joined, f32[8,16]{1,0:T(8,128)} %get-tuple-element.9.decay_in, f32[8,16]{1,0:T(8,128)} %get-tuple-element.10.beta_in, f32[1,16]{1,0:T(1,128)} %bitcast.27, f32[1,16]{1,0:T(1,128)} %bitcast.28, ...), custom_call_target="tpu_custom_call" | custom-call | tf_op jit(solution)/shard_map/pallas_call | solution.py:467
  44.3 35.6 %shard_map.214 = bf16[8,2048]{1,0:T(8,128)(2,1)} custom-call(f32[8,2048]{1,0:T(8,128)} %get-tuple-element.11.branch_ref, bf16[32,8,256]{2,1,0:T(8,128)(2,1)} %get-tuple-element.12.shares_ref, bf16[8,2048]{1,0:T(8,128)(2,1)} %x_hbm.3, f32[1,2048]{1,0:T(1,128)} %bitcast.22, f32[1,2048]{1,0:T(1,128)} %bitcast.23, f32[1,2048]{1,0:T(1,128)} %bitcast.24, ...), custom_call_target="tpu_custom_call" | custom-call | tf_op jit(solution)/shard_map/pallas_call | solution.py:622
  79.9 1.4 %copy.24 = bf16[8,2048]{1,0:T(8,128)(2,1)} copy(bf16[8,2048]{1,0:T(8,128)(2,1)} %shard_map.214) | data formatting | bytes 65536
where the time goes:
time: 81.5 us; the launch traced here: 81.3 us
  Pallas kernels  79.3 us (97%)
  local copies, waits for them, and re-layouts  1.38 us (2%)
    pallas_call x1, Pallas kernels, experts_part(): pl.pallas_call(functools.partial(expert_kernel, devices), out_shape=jax.S...  35.6 us
    pallas_call x1, Pallas kernels, project(): pl.pallas_call(functools.partial(project_kernel, devices, own), out_shape...  27.3 us
    pallas_call x1, Pallas kernels, delta_part(): pl.pallas_call(functools.partial(delta_kernel, own), out_shape=(jax.Shape...  16.3 us

commit v1 on v0

v1 whole, which is shorter than its diff:
```python
import functools
import types

import jax
import jax.numpy as jnp
from jax import lax
from jax.experimental import pallas as pl
from jax.experimental.pallas import tpu as pltpu
from jax.sharding import PartitionSpec as P

H = 16
HD = 128
PIECES = 4
TOPK = 4
LANES = 128
HALF = LANES // 2
VMEM_LIMIT = 58 * 1000 * 1000
MESH = pl.DeviceIdType.MESH

EPS = 1e-06
LIMIT = 7.0
ALPHA = 1.702


def rms_scale(values):
    return values * lax.rsqrt(jnp.mean(values * values, axis=-1, keepdims=True) + EPS)


def clamped_unit(gate, upper):
    glu = jnp.minimum(gate, LIMIT)
    linear = jnp.clip(upper, -LIMIT, LIMIT)
    return glu * jax.nn.sigmoid(ALPHA * glu) * (linear + 1.0)


def flipped(value, distance):
    bit = 1
    while bit <= distance:
        if distance & bit:
            value = value + bit - 2 * bit * (lax.rem(value // bit, 2))
        bit *= 2
    return value


class Place:
    def __init__(self, devices):
        self.layers = devices // 8
        self.me = lax.axis_index("ep")
        self.core = lax.rem(self.me, 2)
        self.x = lax.rem(self.me // 2, 2)
        self.y = lax.rem(self.me // 4, 2)
        self.z = self.me // 8
        self.chip = self.me // 2
        self.partner = flipped(self.me, 1)

    def at(self, distance=0, y=0, x=0):
        z = flipped(self.z, distance)
        return z * 8 + flipped(self.y, y) * 4 + flipped(self.x, x) * 2 + self.core

    def slot(self, distance=0, y=0, x=0):
        return distance * 4 + flipped(self.y, y) * 2 + flipped(self.x, x)


def greet(partners):
    barrier = pltpu.get_barrier_semaphore()
    for partner in partners:
        pl.semaphore_signal(barrier, inc=1, device_id=(partner,), device_id_type=MESH)
    return lambda: pl.semaphore_wait(barrier, len(partners))


def load_all(pairs, sems):
    loads = [
        pltpu.make_async_copy(source, target, sems.at[i])
        for i, (source, target) in enumerate(pairs)
    ]
    for load in loads:
        load.start()
    return loads


def remote(source, target, send_sem, recv_sem, device):
    return pltpu.make_async_remote_copy(
        src_ref=source,
        dst_ref=target,
        send_sem=send_sem,
        recv_sem=recv_sem,
        device_id=(device,),
        device_id_type=MESH,
    )


def gather_sends(devices):
    return 4 * (devices // 8) - 1


PLANE = ((1, 1), (0, 1), (1, 0))


class Gather:
    def __init__(self, place, buf, send_sems, recv_sems):
        self.place, self.buf = place, buf
        self.send_sems, self.recv_sems = send_sems, recv_sems
        self.started = []

    def push(self, source, target, device):
        copy = remote(
            self.buf.at[source],
            self.buf.at[target],
            self.send_sems.at[len(self.started)],
            self.recv_sems.at[target],
            device,
        )
        copy.start()
        self.started.append(copy)

    def arrive(self, slot):
        remote(
            self.buf.at[slot],
            self.buf.at[slot],
            self.send_sems.at[0],
            self.recv_sems.at[slot],
            self.place.partner,
        ).wait_recv()

    def spread(self, distance):
        place = self.place
        slot = place.slot(distance)
        for y, x in PLANE:
            self.push(slot, slot, place.at(y=y, x=x))

    def column(self, distance):
        self.arrive(self.place.slot(distance))
        self.spread(distance)

    def across(self, distance):
        for y, x in reversed(PLANE):
            self.arrive(self.place.slot(distance, y, x))

    def begin(self):
        place = self.place
        for distance in range(1, place.layers):
            self.push(place.slot(), place.slot(distance), place.at(distance))
        self.spread(0)

    def relays(self):
        return [functools.partial(self.column, d) for d in range(1, self.place.layers)]


class Scatter:
    def __init__(self, place, parts, plane, column, sems):
        self.place, self.parts = place, parts
        self.plane, self.column = plane, column
        self.send_sems, self.plane_recv, self.column_recv = sems
        self.started = []
        self.value = None

    def push(self, source, target, recv_sem, device):
        copy = remote(source, target, self.send_sems.at[len(self.started)], recv_sem, device)
        copy.start()
        self.started.append(copy)

    def arrive(self, target, recv_sem):
        remote(target, target, self.send_sems.at[0], recv_sem, self.place.partner).wait_recv()

    def first(self, distance):
        place = self.place
        for i, (y, x) in enumerate(PLANE):
            at = 3 * distance + i
            self.push(
                self.parts.at[place.slot(distance, y, x)],
                self.plane.at[at],
                self.plane_recv.at[at],
                place.at(y=y, x=x),
            )

    def last(self, distance):
        place = self.place
        slot = place.slot(distance)
        value = wide(self.parts[slot])
        for i in reversed(range(3)):
            at = 3 * distance + i
            self.arrive(self.plane.at[at], self.plane_recv.at[at])
            value = value + wide(self.plane[at])
        if distance > 0:
            self.parts[slot] = value.astype(jnp.bfloat16)
            self.push(
                self.parts.at[slot],
                self.column.at[distance],
                self.column_recv.at[distance],
                place.at(distance),
            )
        else:
            self.value = value

    def collect(self, distance):
        self.arrive(self.column.at[distance], self.column_recv.at[distance])
        self.value = self.value + wide(self.column[distance])


def settle(started):
    for copy in started:
        copy.wait_send()


def wide(block):
    return block.astype(jnp.float32)


def dot_t(left, right):
    return lax.dot_general(
        left, right, (((1,), (1,)), ((), ())), preferred_element_type=jnp.float32
    )


def column_of(row):
    size = row.shape[1]
    across = lax.broadcasted_iota(jnp.int32, (size, size), 1)
    down = lax.broadcasted_iota(jnp.int32, (size, size), 0)
    return jnp.sum(
        jnp.where(across == down, jnp.broadcast_to(row, (size, size)), 0.0), axis=1, keepdims=True
    )


def share_rows(routes, logits):
    raised = jnp.exp(logits)
    shares = raised / jnp.sum(raised, axis=0, keepdims=True)
    routes = routes.astype(jnp.float32)
    count = routes.shape[1]
    lane = lax.broadcasted_iota(jnp.int32, (count, LANES), 1)
    expert = lax.rem(lane, HALF).astype(jnp.float32)
    share = jnp.zeros((count, LANES), jnp.float32)
    for j in range(routes.shape[0]):
        share = share + jnp.where(
            expert == column_of(routes[j : j + 1]), column_of(shares[j : j + 1]), 0.0
        )
    high = share.astype(jnp.bfloat16)
    low = (share - wide(high)).astype(jnp.bfloat16)
    return jnp.where(lane < HALF, wide(high), wide(low)).astype(jnp.bfloat16)


def head_rows(joined, head, kind, piece):
    lane = lax.broadcasted_iota(jnp.int32, (joined.shape[1], LANES), 1)
    value = jnp.zeros(lane.shape, jnp.float32)
    group, offset = divmod(kind * piece, LANES)
    for i in range(HD // piece):
        part = joined[head * (HD // piece) + i, :, group * LANES : (group + 1) * LANES]
        part = wide(part)
        shift = (i * piece - offset) % LANES
        if shift:
            part = pltpu.roll(part, shift, 1)
        value = jnp.where((lane >= i * piece) & (lane < (i + 1) * piece), part, value)
    return value


def all_heads(joined, heads, kind, piece):
    if piece == HD:
        return wide(joined[:, :, kind * HD : (kind + 1) * HD])
    return jnp.stack([head_rows(joined, head, kind, piece) for head in range(heads)])


def inverse_norm(values):
    return lax.rsqrt(jnp.sum(values * values, axis=-1, keepdims=True) + EPS)


INPUTS = (
    "x",
    "gain",
    "routes",
    "logits",
    "w_decay",
    "w_beta",
    "scale",
    "bias",
    "head_gain",
    "gain_mix",
    "gain_pre",
    "gain_post",
    "query",
    "key",
    "value",
    "outgate",
    "state",
    "w_out",
    "gate",
    "up",
    "down",
)
SMALL = INPUTS[:12]


def decode_kernel(devices, names, *refs):
    r = types.SimpleNamespace(**dict(zip(names, refs)))
    place = Place(devices)
    layers, pairs = place.layers, devices // 2
    core, other = place.core, 1 - place.core
    count, width = r.x.shape
    heads = r.keys.shape[0]
    piece = 2 * r.query_hbm.shape[0]
    hidden_units = r.gate_hbm.shape[1]
    half = max(1, layers // 2)
    chunks = [c for c in (range(0, half), range(half, layers)) if len(c)]

    ready = greet(
        [place.at(distance) for distance in range(1, layers)]
        + [place.at(y=y, x=x) for y, x in PLANE]
        + [place.partner]
    )
    loads = load_all(
        [(getattr(r, name + "_hbm"), getattr(r, name)) for name in SMALL], r.small_sems
    )
    projections = (r.query_hbm, r.key_hbm, r.value_hbm, r.outgate_hbm)
    experts = ((r.gate_hbm, r.gate), (r.up_hbm, r.up), (r.down_hbm, r.down))
    weight_loads = load_all(
        [(ref, r.weights.at[i, core]) for i, ref in enumerate(projections)], r.weight_sems
    )
    loads[0].wait()
    loads[1].wait()
    normed = (rms_scale(wide(r.x[...])) * r.gain[...]).astype(jnp.bfloat16)
    gather = Gather(place, r.rows_one, r.one_send, r.one_recv)
    r.rows_one[place.slot()] = normed
    ready()
    gather.begin()
    swaps = [
        remote(
            ref, r.weights.at[i, core], r.swap_send.at[i], r.swap_recv.at[i], place.partner
        )
        for i, ref in enumerate(projections)
    ]
    for swap in swaps:
        swap.start()
    late_loads = load_all(
        [(r.state_hbm, r.state), (r.w_out_hbm, r.w_out)]
        + [(ref, into.at[core]) for ref, into in experts],
        r.late_sems,
    )
    for step in gather.relays():
        step()
    sent = []
    for number, chunk in enumerate(chunks):
        for distance in chunk:
            gather.across(distance)
        if not number:
            for load in weight_loads:
                load.wait()
            for i, ref in enumerate(projections):
                remote(
                    ref,
                    r.weights.at[i, other],
                    r.swap_send.at[i],
                    r.swap_recv.at[i],
                    place.partner,
                ).wait_recv()
        a, b = 4 * chunk[0], 4 * (chunk[-1] + 1)
        rows = r.rows_one[a:b].reshape((b - a) * count, width)
        weights = r.weights[...].reshape(4 * piece, width)
        r.columns[a:b] = dot_t(rows, weights).astype(jnp.bfloat16).reshape(b - a, count, 4 * piece)
        for distance in reversed(chunk):
            for y, x in ((1, 1), (0, 1), (1, 0), (0, 0)):
                if (distance, y, x) == (0, 0, 0):
                    r.joined[place.chip] = r.columns[place.slot()]
                    continue
                copy = remote(
                    r.columns.at[place.slot(distance, y, x)],
                    r.joined.at[place.chip],
                    r.out_sems.at[len(sent)],
                    r.in_sems.at[place.chip],
                    place.at(distance, y, x),
                )
                copy.start()
                sent.append(copy)
    expert_swaps = [
        remote(ref, into.at[core], r.swap_send.at[4 + i], r.swap_recv.at[4 + i], place.partner)
        for i, (ref, into) in enumerate(experts)
    ]
    for swap in expert_swaps:
        swap.start()
    for load in loads[2:]:
        load.wait()
    decay = jnp.exp(
        -r.scale[...] * jax.nn.softplus(dot_t(normed, r.w_decay[...]) + r.bias[...])
    )
    strength = jax.nn.sigmoid(dot_t(normed, r.w_beta[...]))
    for h in range(heads):
        r.keep[h] = jnp.broadcast_to(decay[:, h : h + 1], (count, HD))
        r.beta[h] = jnp.broadcast_to(strength[:, h : h + 1], (count, HD))
    r.rows_two[place.slot(), :, width:] = share_rows(r.routes[...], r.logits[...])
    late_loads[0].wait()
    late_loads[1].wait()
    group = heads // layers
    down = lax.broadcasted_iota(jnp.int32, (count, HD), 0)
    for distance in range(layers):
        layer = flipped(place.z, distance)
        for y, x in ((0, 0), (0, 1), (1, 0), (1, 1)):
            if (distance, y, x) != (0, 0, 0):
                source = place.at(distance, y, x) // 2
                remote(
                    r.columns.at[0],
                    r.joined.at[source],
                    r.out_sems.at[0],
                    r.in_sems.at[source],
                    place.partner,
                ).wait_recv()
        own_heads = pl.ds(group * layer, group)
        joined = r.joined.at[pl.ds(4 * layer, 4)]
        query = jax.nn.silu(all_heads(joined, group, 0, piece))
        query = query * inverse_norm(query) * HD ** (-0.5)
        keys = jax.nn.silu(all_heads(joined, group, 1, piece))
        keys = keys * inverse_norm(keys)
        r.keys[own_heads] = keys
        asks = jnp.concatenate([keys, query], axis=1).astype(jnp.bfloat16)
        overlap = jnp.sum(keys * query, axis=-1, keepdims=True)
        guesses, sights = [], []
        for h in range(group):
            guess = jnp.zeros((count, HD), jnp.float32)
            seen = jnp.zeros((count, HD), jnp.float32)
            for i in range(count):
                both = jnp.dot(
                    asks[h], r.state[i, group * layer + h], preferred_element_type=jnp.float32
                )
                guess = jnp.where(down == i, both[0:count], guess)
                seen = jnp.where(down == i, both[count:], seen)
            guesses.append(guess)
            sights.append(seen)
        keep = r.keep[own_heads]
        values = jax.nn.silu(all_heads(joined, group, 2, piece))
        change = r.beta[own_heads] * (values - keep * jnp.stack(guesses))
        r.change[own_heads] = change
        output = rms_scale(keep * jnp.stack(sights) + overlap * change) * r.head_gain[...]
        mixed = (output * jax.nn.silu(all_heads(joined, group, 3, piece))).astype(jnp.bfloat16)
        mixed = jnp.concatenate([mixed[h] for h in range(group)], axis=1)
        rows = pl.ds(pl.multiple_of(group * HD * layer, HD), group * HD)
        for j in range(0, width, 512):
            branch = jnp.dot(
                mixed, r.w_out[rows, j : j + 512], preferred_element_type=jnp.float32
            )
            if distance:
                branch = branch + r.x_second[:, j : j + 512]
            r.x_second[:, j : j + 512] = branch
    x_second = wide(r.x[...]) + rms_scale(r.x_second[...]) * r.gain_mix[...]
    r.x_second[...] = x_second
    r.rows_two[place.slot(), :, 0:width] = (rms_scale(x_second) * r.gain_pre[...]).astype(
        jnp.bfloat16
    )
    second = Gather(place, r.rows_two, r.two_send, r.two_recv)
    second.begin()

    def update(h, carry):
        upright = jnp.transpose(r.keys[h])
        change, keep = r.change[h], r.keep[h]
        for i in range(count):
            held = wide(r.state[i, h])
            key = jnp.broadcast_to(upright[:, i : i + 1], held.shape)
            r.new_state[i, h] = (keep[i : i + 1] * held + key * change[i : i + 1]).astype(
                jnp.bfloat16
            )
        return carry

    scatter = Scatter(
        place,
        r.parts,
        r.plane,
        r.column,
        (r.sum_send, r.plane_recv, r.column_recv),
    )
    plan = [heads * i // 16 for i in (0, 5, 11, 14, 16)]

    def fill(i):
        lax.fori_loop(plan[i], plan[i + 1], update, 0)

    fill(0)
    for step in second.relays():
        step()
    fill(1)

    def compute(chunk):
        a, b = 4 * chunk[0], 4 * (chunk[-1] + 1)
        number = (b - a) * count

        rows = r.rows_two[a:b, :, 0:width].reshape(number, width)
        share = wide(r.rows_two[a:b, :, width:]).reshape(number, LANES)
        lane = lax.rem(lax.broadcasted_iota(jnp.int32, share.shape, 1), HALF)
        share = jnp.sum(jnp.where(lane == place.me // PIECES, share, 0.0), axis=1, keepdims=True)
        for i in range(2):
            for j in range(0, hidden_units, 256):
                gated = clamped_unit(
                    jnp.dot(rows, r.gate[i, :, j : j + 256], preferred_element_type=jnp.float32),
                    jnp.dot(rows, r.up[i, :, j : j + 256], preferred_element_type=jnp.float32),
                )
                at = i * hidden_units + j
                r.hidden[0:number, at : at + 256] = gated.astype(jnp.bfloat16)
        units = r.hidden[0:number]
        for j in range(0, width, 512):
            weights = r.down[:, :, j : j + 512].reshape(2 * hidden_units, 512)
            part = jnp.dot(units, weights, preferred_element_type=jnp.float32)
            r.parts[a:b, :, j : j + 512] = (
                (part * share).astype(jnp.bfloat16).reshape(b - a, count, 512)
            )
        for distance in reversed(chunk):
            scatter.first(distance)

    for number, chunk in enumerate(chunks):
        for distance in chunk:
            second.across(distance)
        if not number:
            for load in late_loads[2:]:
                load.wait()
            for i, (ref, into) in enumerate(experts):
                remote(
                    ref, into.at[other], r.swap_send.at[4 + i], r.swap_recv.at[4 + i], place.partner
                ).wait_recv()
        compute(chunk)
    fill(2)
    for chunk in chunks:
        for distance in reversed(chunk):
            scatter.last(distance)
    fill(3)
    for distance in range(1, layers):
        scatter.collect(distance)
    r.result[...] = (r.x_second[...] + rms_scale(scatter.value) * r.gain_post[...]).astype(
        jnp.bfloat16
    )
    settle(
        gather.started + swaps + sent + expert_swaps + second.started + scatter.started
    )


def store_kernel(result, new_state, result_hbm, state_hbm, sems):
    pairs = [(new_state.at[i], state_hbm.at[i]) for i in range(new_state.shape[0])]
    for store in load_all([(result, result_hbm)] + pairs, sems):
        store.wait()


def shards(
    residual_in,
    gain_mix_pre,
    w_query,
    w_key,
    w_value,
    w_outgate,
    w_decay,
    w_beta,
    decay_scale,
    decay_bias,
    head_gain,
    w_out,
    gain_mix_post,
    state_cache,
    gain_ffn_pre,
    routes,
    route_logits,
    w_gate,
    w_up,
    w_down,
    gain_ffn_post,
):
    devices = lax.axis_size("ep")
    layers, pairs = devices // 8, devices // 2
    count, width = residual_in.shape
    heads = w_decay.shape[1]
    own = w_query.shape[1]
    units = w_gate.shape[1]
    rows = 4 * max(1, layers // 2) * count
    if layers > 1:
        rows = max(rows, 4 * (layers - layers // 2) * count)
    inputs = dict(
        x=residual_in,
        gain=gain_mix_pre[None],
        routes=routes.T,
        logits=route_logits.T,
        w_decay=w_decay.T,
        w_beta=w_beta.T,
        scale=decay_scale[None],
        bias=decay_bias[None],
        head_gain=head_gain[None],
        gain_mix=gain_mix_post[None],
        gain_pre=gain_ffn_pre[None],
        gain_post=gain_ffn_post[None],
        query=w_query.T,
        key=w_key.T,
        value=w_value.T,
        outgate=w_outgate.T,
        state=state_cache,
        w_out=w_out,
        gate=w_gate,
        up=w_up,
        down=w_down,
    )
    bf16, f32 = jnp.bfloat16, jnp.float32
    dma = pltpu.SemaphoreType.DMA

    def blocks(number, lanes=width):
        return pltpu.VMEM((number, count, lanes), bf16)

    def per_head():
        return pltpu.VMEM((heads, count, HD), f32)

    scratch = {name: pltpu.VMEM(inputs[name].shape, inputs[name].dtype) for name in SMALL}
    scratch |= dict(
        weights=pltpu.VMEM((4, 2, own, width), bf16),
        state=pltpu.VMEM(state_cache.shape, bf16),
        w_out=pltpu.VMEM(w_out.shape, bf16),
        gate=pltpu.VMEM((2,) + w_gate.shape, bf16),
        up=pltpu.VMEM((2,) + w_up.shape, bf16),
        down=pltpu.VMEM((2,) + w_down.shape, bf16),
        rows_one=blocks(pairs),
        rows_two=blocks(pairs, width + LANES),
        columns=blocks(pairs, 8 * own),
        joined=blocks(pairs, 8 * own),
        keys=per_head(),
        keep=per_head(),
        beta=per_head(),
        change=per_head(),
        x_second=pltpu.VMEM((count, width), f32),
        hidden=pltpu.VMEM((rows, 2 * units), bf16),
        parts=blocks(pairs),
        plane=blocks(3 * layers),
        column=blocks(layers),
        small_sems=dma((len(SMALL),)),
        weight_sems=dma((4,)),
        late_sems=dma((5,)),
        swap_send=dma((7,)),
        swap_recv=dma((7,)),
        one_send=dma((gather_sends(devices),)),
        one_recv=dma((pairs,)),
        two_send=dma((gather_sends(devices),)),
        two_recv=dma((pairs,)),
        out_sems=dma((pairs,)),
        in_sems=dma((pairs,)),
        sum_send=dma((4 * layers,)),
        plane_recv=dma((3 * layers,)),
        column_recv=dma((layers,)),
    )
    names = [name + "_hbm" for name in INPUTS] + ["result", "new_state"] + list(scratch)
    vmem = pl.BlockSpec(memory_space=pltpu.VMEM)
    hbm = pl.BlockSpec(memory_space=pltpu.HBM)
    held = pl.pallas_call(
        functools.partial(decode_kernel, devices, names),
        out_shape=(
            pltpu.VMEM((count, width), bf16),
            pltpu.VMEM(state_cache.shape, bf16),
        ),
        in_specs=[hbm] * len(INPUTS),
        out_specs=(vmem, vmem),
        scratch_shapes=list(scratch.values()),
        compiler_params=pltpu.CompilerParams(
            collective_id=0, has_side_effects=True, vmem_limit_bytes=VMEM_LIMIT
        ),
    )(*[inputs[name] for name in INPUTS])
    return pl.pallas_call(
        store_kernel,
        out_shape=[jax.ShapeDtypeStruct(a.shape, a.dtype) for a in held],
        in_specs=[vmem] * 2,
        out_specs=[hbm] * 2,
        scratch_shapes=[dma((count + 1,))],
        compiler_params=pltpu.CompilerParams(vmem_limit_bytes=1000 * 1000),
    )(*held)


def solution(mesh):
    in_specs = (
        P("ep", None),
        P(),
        P(None, "ep"),
        P(None, "ep"),
        P(None, "ep"),
        P(None, "ep"),
        P(),
        P(),
        P(),
        P(),
        P(),
        P(),
        P(),
        P("ep", None, None, None),
        P(),
        P("ep", None),
        P("ep", None),
        P(None, "ep"),
        P(None, "ep"),
        P("ep", None),
        P(),
    )
    out_specs = (P("ep", None), P("ep", None, None, None))
    return jax.shard_map(shards, mesh=mesh, in_specs=in_specs, out_specs=out_specs, check_vma=False)
```

time: 81.5 us -> 45.3 us (0.56)
  Pallas kernels: 79.3 us -> 44.5 us
  local copies, waits for them, and re-layouts: 1.38 us -> 0 us
    pallas_call x3 -> x2, Pallas kernels: 79.3 us -> 44.5 us  [the longest x1 42.4 us: shards(): pl.pallas_call(functools.partial(decode_kernel, devices, names), out_shap...]
    unnamed x1 -> x0, local copies, waits for them, and re-layouts: 1.38 us -> none
where the time goes in v1:
time: 45.3 us; the launch traced here: 45.1 us
  Pallas kernels  44.5 us (98%)
  between operations  0.65 us (1%)
    pallas_call x1, Pallas kernels, shards(): pl.pallas_call(functools.partial(decode_kernel, devices, names), out_shap...  42.4 us
    pallas_call x1, Pallas kernels, shards(): pl.pallas_call(store_kernel, out_shape=[jax.ShapeDtypeStruct(a.shape, a.d...  2.09 us

profile of v1, /device:TPU:0, one launch (start us, length us, event | category | flops | bytes accessed | tf_op | source)
XLA Modules:
  0.0 45.1 jit_solution(2203201475091434775)
XLA Ops:
  0.6 42.4 %shard_map.212 = (bf16[8,2048]{1,0:T(8,128)(2,1)S(1)}, bf16[8,16,128,128]{3,2,1,0:T(8,128)(2,1)S(1)}) custom-call(bf16[8,2048]{1,0:T(8,128)(2,1)} %refs_0_.1, f32[1,2048]{1,0:T(1,128)} %bitcast.21, s32[4,8]{1,0:T(4,128)} %bitcast.25, f32[4,8]{1,0:T(4,128)} %bitcast.26, bf16[16,2048]{1,0:T(8,128)(2,1)} %bitcast.19, bf16[16,2048]{1,0:T(8,128)(2,1)} %bitcast.20, ...), custom_call_target="tpu_custom_call" | custom-call | tf_op jit(solution)/shard_map/pallas_call | solution.py:635
  43.0 2.1 %shard_map.213 = (bf16[8,2048]{1,0:T(8,128)(2,1)}, bf16[8,16,128,128]{3,2,1,0:T(8,128)(2,1)}) custom-call(bf16[8,2048]{1,0:T(8,128)(2,1)S(1)} %get-tuple-element.4.result, bf16[8,16,128,128]{3,2,1,0:T(8,128)(2,1)S(1)} %get-tuple-element.5.new_state), custom_call_target="tpu_custom_call" | custom-call | tf_op jit(solution)/shard_map/pallas_call | solution.py:648

commit v2 on v1

v2 whole, which is shorter than its diff:
```python
import functools
import types

import jax
import jax.numpy as jnp
from jax import lax
from jax.experimental import pallas as pl
from jax.experimental.pallas import tpu as pltpu
from jax.sharding import PartitionSpec as P

H = 16
HD = 128
PIECES = 4
TOPK = 4
LANES = 128
HALF = LANES // 2
SUM_CUTS = 2
VMEM_LIMIT = 58 * 1000 * 1000
MESH = pl.DeviceIdType.MESH

EPS = 1e-06
LIMIT = 7.0
ALPHA = 1.702


def rms_scale(values):
    return values * lax.rsqrt(jnp.mean(values * values, axis=-1, keepdims=True) + EPS)


def clamped_unit(gate, upper):
    glu = jnp.minimum(gate, LIMIT)
    linear = jnp.clip(upper, -LIMIT, LIMIT)
    return glu * jax.nn.sigmoid(ALPHA * glu) * (linear + 1.0)


def flipped(value, distance):
    bit = 1
    while bit <= distance:
        if distance & bit:
            value = value + bit - 2 * bit * (lax.rem(value // bit, 2))
        bit *= 2
    return value


class Place:
    def __init__(self, devices):
        self.layers = devices // 8
        self.me = lax.axis_index("ep")
        self.core = lax.rem(self.me, 2)
        self.x = lax.rem(self.me // 2, 2)
        self.y = lax.rem(self.me // 4, 2)
        self.z = self.me // 8
        self.chip = self.me // 2
        self.partner = flipped(self.me, 1)

    def at(self, distance=0, y=0, x=0):
        z = flipped(self.z, distance)
        return z * 8 + flipped(self.y, y) * 4 + flipped(self.x, x) * 2 + self.core

    def slot(self, distance=0, y=0, x=0):
        return distance * 4 + flipped(self.y, y) * 2 + flipped(self.x, x)


def greet(partners):
    barrier = pltpu.get_barrier_semaphore()
    for partner in partners:
        pl.semaphore_signal(barrier, inc=1, device_id=(partner,), device_id_type=MESH)
    return lambda: pl.semaphore_wait(barrier, len(partners))


def remote(source, target, send_sem, recv_sem, device):
    return pltpu.make_async_remote_copy(
        src_ref=source,
        dst_ref=target,
        send_sem=send_sem,
        recv_sem=recv_sem,
        device_id=(device,),
        device_id_type=MESH,
    )


PLANE = ((1, 1), (0, 1), (1, 0))


def lanes_of(ref, cuts):
    width = ref.shape[-1]
    bounds = [width // LANES * i // cuts * LANES for i in range(cuts + 1)]
    return [pl.ds(a, b - a) for a, b in zip(bounds, bounds[1:])]


def chunks_of(layers):
    half = max(1, layers // 2)
    return [c for c in (range(0, half), range(half, layers)) if len(c)]


class Gather:
    def __init__(self, place, buf, send_sem, column_recv, plane_recv):
        self.place, self.buf = place, buf
        self.send_sem, self.column_recv, self.plane_recv = send_sem, column_recv, plane_recv
        self.sends = 0
        self.chunks = chunks_of(place.layers)

    def push(self, source, target, recv_sem, device):
        remote(
            self.buf.at[source], self.buf.at[target], self.send_sem.at[0], recv_sem, device
        ).start()
        self.sends += 1

    def arrive(self, blocks, recv_sem):
        remote(blocks, blocks, self.send_sem.at[0], recv_sem, self.place.partner).wait_recv()

    def spread(self, distance):
        place = self.place
        slot = place.slot(distance)
        sem = self.plane_recv.at[[distance in chunk for chunk in self.chunks].index(True)]
        for y, x in PLANE:
            self.push(slot, slot, sem, place.at(y=y, x=x))

    def column(self, distance):
        slot = self.place.slot(distance)
        self.arrive(self.buf.at[slot], self.column_recv.at[distance])
        self.spread(distance)

    def across(self, number):
        blocks = 3 * len(self.chunks[number])
        self.arrive(self.buf.at[pl.ds(0, blocks)], self.plane_recv.at[number])

    def begin(self):
        place = self.place
        for distance in range(1, place.layers):
            self.push(
                place.slot(),
                place.slot(distance),
                self.column_recv.at[distance],
                place.at(distance),
            )
        self.spread(0)

    def relays(self):
        return [functools.partial(self.column, d) for d in range(1, self.place.layers)]

    def settle(self):
        settle(self.buf.at[pl.ds(0, self.sends)], self.send_sem.at[0], self.place.partner)


class Scatter:
    def __init__(self, place, parts, plane, column, cuts, sems):
        self.place, self.parts = place, parts
        self.plane, self.column = plane, column
        self.lanes = lanes_of(parts, cuts)
        self.send_sem, self.plane_recv, self.column_recv = sems
        self.sends = 0
        self.values = [None] * cuts

    def push(self, source, target, recv_sem, device):
        remote(source, target, self.send_sem.at[0], recv_sem, device).start()
        self.sends += 1

    def arrive(self, blocks, recv_sem):
        remote(blocks, blocks, self.send_sem.at[0], recv_sem, self.place.partner).wait_recv()

    def first(self, distance, cut):
        place, lanes = self.place, self.lanes[cut]
        for i, (y, x) in enumerate(PLANE):
            self.push(
                self.parts.at[place.slot(distance, y, x), :, lanes],
                self.plane.at[3 * distance + i, :, lanes],
                self.plane_recv.at[distance, cut],
                place.at(y=y, x=x),
            )

    def last(self, distance, cut):
        place, lanes = self.place, self.lanes[cut]
        slot = place.slot(distance)
        value = wide(self.parts[slot, :, lanes])
        self.arrive(
            self.plane.at[pl.ds(3 * distance, 3), :, lanes], self.plane_recv.at[distance, cut]
        )
        for i in reversed(range(3)):
            value = value + wide(self.plane[3 * distance + i, :, lanes])
        if distance > 0:
            self.parts[slot, :, lanes] = value.astype(jnp.bfloat16)
            self.push(
                self.parts.at[slot, :, lanes],
                self.column.at[distance - 1, :, lanes],
                self.column_recv.at[cut],
                place.at(distance),
            )
        else:
            self.values[cut] = value

    def collect(self, cut):
        lanes = self.lanes[cut]
        others = self.place.layers - 1
        if others:
            self.arrive(self.column.at[pl.ds(0, others), :, lanes], self.column_recv.at[cut])
        for i in range(others):
            self.values[cut] = self.values[cut] + wide(self.column[i, :, lanes])

    def settle(self):
        blocks = self.sends // len(self.lanes)
        settle(self.parts.at[pl.ds(0, blocks)], self.send_sem.at[0], self.place.partner)


def settle(blocks, send_sem, partner):
    remote(blocks, blocks, send_sem, send_sem, partner).wait_send()


def landed(blocks, sem):
    pltpu.make_async_copy(blocks, blocks, sem).wait()


def wide(block):
    return block.astype(jnp.float32)


def dot_t(left, right):
    return lax.dot_general(
        left, right, (((1,), (1,)), ((), ())), preferred_element_type=jnp.float32
    )


def column_of(row):
    size = row.shape[1]
    across = lax.broadcasted_iota(jnp.int32, (size, size), 1)
    down = lax.broadcasted_iota(jnp.int32, (size, size), 0)
    return jnp.sum(
        jnp.where(across == down, jnp.broadcast_to(row, (size, size)), 0.0), axis=1, keepdims=True
    )


def share_rows(routes, logits):
    raised = jnp.exp(logits)
    shares = raised / jnp.sum(raised, axis=0, keepdims=True)
    routes = routes.astype(jnp.float32)
    count = routes.shape[1]
    lane = lax.broadcasted_iota(jnp.int32, (count, LANES), 1)
    expert = lax.rem(lane, HALF).astype(jnp.float32)
    share = jnp.zeros((count, LANES), jnp.float32)
    for j in range(routes.shape[0]):
        share = share + jnp.where(
            expert == column_of(routes[j : j + 1]), column_of(shares[j : j + 1]), 0.0
        )
    high = share.astype(jnp.bfloat16)
    low = (share - wide(high)).astype(jnp.bfloat16)
    return jnp.where(lane < HALF, wide(high), wide(low)).astype(jnp.bfloat16)


def head_rows(joined, head, kind, piece):
    lane = lax.broadcasted_iota(jnp.int32, (joined.shape[1], LANES), 1)
    value = jnp.zeros(lane.shape, jnp.float32)
    group, offset = divmod(kind * piece, LANES)
    for i in range(HD // piece):
        part = joined[head * (HD // piece) + i, :, group * LANES : (group + 1) * LANES]
        part = wide(part)
        shift = (i * piece - offset) % LANES
        if shift:
            part = pltpu.roll(part, shift, 1)
        value = jnp.where((lane >= i * piece) & (lane < (i + 1) * piece), part, value)
    return value


def all_heads(joined, heads, kind, piece):
    if piece == HD:
        return wide(joined[:, :, kind * HD : (kind + 1) * HD])
    return jnp.stack([head_rows(joined, head, kind, piece) for head in range(heads)])


def inverse_norm(values):
    return lax.rsqrt(jnp.sum(values * values, axis=-1, keepdims=True) + EPS)


GROUPS = dict(
    x=("x",),
    gain=("gain",),
    routes=("routes",),
    logits=("logits",),
    rates=("w_decay", "w_beta"),
    decays=("scale", "bias"),
    head_gain=("head_gain",),
    gains=("gain_mix", "gain_pre", "gain_post"),
    weights=("query", "key", "value", "outgate"),
    state=("state",),
    w_out=("w_out",),
    wide_in=("gate", "up"),
    down=("down",),
)
INPUTS = tuple(name for group in GROUPS.values() for name in group)
PAIRED = ("weights", "wide_in", "down")
LATE = ("state", "w_out", "wide_in", "down")


def decode_kernel(devices, names, *refs):
    r = types.SimpleNamespace(**dict(zip(names, refs)))
    place = Place(devices)
    layers, pairs = place.layers, devices // 2
    core, other = place.core, 1 - place.core
    count, width = r.x.shape
    heads = r.keys.shape[0]
    piece = 2 * r.query_hbm.shape[0]
    hidden_units = r.gate_hbm.shape[1]
    chunks = chunks_of(layers)

    def target(group, i):
        into = getattr(r, group)
        if group in PAIRED:
            return into.at[i, core]
        return into if len(GROUPS[group]) == 1 else into.at[i]

    def load(groups):
        for group in groups:
            for i, name in enumerate(GROUPS[group]):
                pltpu.make_async_copy(
                    getattr(r, name + "_hbm"), target(group, i), r.load_sems.at[order[group]]
                ).start()

    def loaded(group):
        into = getattr(r, group)
        landed(into.at[:, core] if group in PAIRED else into, r.load_sems.at[order[group]])

    def swap(group):
        for i, name in enumerate(GROUPS[group]):
            at = PAIRED.index(group)
            remote(
                getattr(r, name + "_hbm"),
                target(group, i),
                r.swap_send.at[at],
                r.swap_recv.at[at],
                place.partner,
            ).start()

    def swapped(group):
        at = PAIRED.index(group)
        into = getattr(r, group).at[:, other]
        remote(into, into, r.swap_send.at[at], r.swap_recv.at[at], place.partner).wait_recv()

    def swaps_settle(groups):
        for group in groups:
            into = getattr(r, group).at[:, core]
            settle(into, r.swap_send.at[PAIRED.index(group)], place.partner)

    order = {group: i for i, group in enumerate(GROUPS)}
    ready = greet(
        [place.at(distance) for distance in range(1, layers)]
        + [place.at(y=y, x=x) for y, x in PLANE]
        + [place.partner]
    )
    load(group for group in GROUPS if group not in LATE)
    loaded("x")
    loaded("gain")
    normed = (rms_scale(wide(r.x[...])) * r.gain[...]).astype(jnp.bfloat16)
    gather = Gather(place, r.rows_one, r.one_send, r.one_column, r.one_plane)
    r.rows_one[place.slot()] = normed
    ready()
    gather.begin()
    swap("weights")
    load(LATE)
    for step in gather.relays():
        step()
    for number, chunk in enumerate(chunks):
        gather.across(number)
        if not number:
            loaded("weights")
            swapped("weights")
        a, b = 4 * chunk[0], 4 * (chunk[-1] + 1)
        rows = r.rows_one[a:b].reshape((b - a) * count, width)
        weights = r.weights[...].reshape(4 * piece, width)
        r.columns[a:b] = dot_t(rows, weights).astype(jnp.bfloat16).reshape(b - a, count, 4 * piece)
        for distance in reversed(chunk):
            for y, x in ((1, 1), (0, 1), (1, 0), (0, 0)):
                if (distance, y, x) == (0, 0, 0):
                    r.joined[place.chip] = r.columns[place.slot()]
                    continue
                remote(
                    r.columns.at[place.slot(distance, y, x)],
                    r.joined.at[place.chip],
                    r.out_sem.at[0],
                    r.in_sems.at[distance],
                    place.at(distance, y, x),
                ).start()
    swap("wide_in")
    swap("down")
    for group in ("routes", "logits", "rates", "decays", "head_gain", "gains"):
        loaded(group)
    decay = jnp.exp(
        -r.decays[0] * jax.nn.softplus(dot_t(normed, r.rates[0]) + r.decays[1])
    )
    strength = jax.nn.sigmoid(dot_t(normed, r.rates[1]))
    for h in range(heads):
        r.keep[h] = jnp.broadcast_to(decay[:, h : h + 1], (count, HD))
        r.beta[h] = jnp.broadcast_to(strength[:, h : h + 1], (count, HD))
    r.rows_two[place.slot(), :, width:] = share_rows(r.routes[...], r.logits[...])
    loaded("state")
    loaded("w_out")
    group = heads // layers
    down = lax.broadcasted_iota(jnp.int32, (count, HD), 0)
    for distance in range(layers):
        layer = flipped(place.z, distance)
        blocks = r.joined.at[pl.ds(0, 4 if distance else 3)]
        remote(
            blocks, blocks, r.out_sem.at[0], r.in_sems.at[distance], place.partner
        ).wait_recv()
        own_heads = pl.ds(group * layer, group)
        joined = r.joined.at[pl.ds(4 * layer, 4)]
        query = jax.nn.silu(all_heads(joined, group, 0, piece))
        query = query * inverse_norm(query) * HD ** (-0.5)
        keys = jax.nn.silu(all_heads(joined, group, 1, piece))
        keys = keys * inverse_norm(keys)
        r.keys[own_heads] = keys
        asks = jnp.concatenate([keys, query], axis=1).astype(jnp.bfloat16)
        overlap = jnp.sum(keys * query, axis=-1, keepdims=True)
        guesses, sights = [], []
        for h in range(group):
            guess = jnp.zeros((count, HD), jnp.float32)
            seen = jnp.zeros((count, HD), jnp.float32)
            for i in range(count):
                both = jnp.dot(
                    asks[h], r.state[i, group * layer + h], preferred_element_type=jnp.float32
                )
                guess = jnp.where(down == i, both[0:count], guess)
                seen = jnp.where(down == i, both[count:], seen)
            guesses.append(guess)
            sights.append(seen)
        keep = r.keep[own_heads]
        values = jax.nn.silu(all_heads(joined, group, 2, piece))
        change = r.beta[own_heads] * (values - keep * jnp.stack(guesses))
        r.change[own_heads] = change
        output = rms_scale(keep * jnp.stack(sights) + overlap * change) * r.head_gain[...]
        mixed = (output * jax.nn.silu(all_heads(joined, group, 3, piece))).astype(jnp.bfloat16)
        mixed = jnp.concatenate([mixed[h] for h in range(group)], axis=1)
        rows = pl.ds(pl.multiple_of(group * HD * layer, HD), group * HD)
        for j in range(0, width, 512):
            branch = jnp.dot(
                mixed, r.w_out[rows, j : j + 512], preferred_element_type=jnp.float32
            )
            if distance:
                branch = branch + r.x_second[:, j : j + 512]
            r.x_second[:, j : j + 512] = branch
    x_second = wide(r.x[...]) + rms_scale(r.x_second[...]) * r.gains[0]
    r.x_second[...] = x_second
    r.rows_two[place.slot(), :, 0:width] = (rms_scale(x_second) * r.gains[1]).astype(
        jnp.bfloat16
    )
    second = Gather(place, r.rows_two, r.two_send, r.two_column, r.two_plane)
    second.begin()

    def update(h, carry):
        upright = jnp.transpose(r.keys[h])
        change, keep = r.change[h], r.keep[h]
        for i in range(count):
            held = wide(r.state[i, h])
            key = jnp.broadcast_to(upright[:, i : i + 1], held.shape)
            r.new_state[i, h] = (keep[i : i + 1] * held + key * change[i : i + 1]).astype(
                jnp.bfloat16
            )
        return carry

    scatter = Scatter(
        place,
        r.parts,
        r.plane,
        r.column,
        SUM_CUTS,
        (r.sum_send, r.plane_recv, r.column_recv),
    )
    plan = [heads * i // 16 for i in (0, 5, 9, 13, 16)]

    def fill(i):
        lax.fori_loop(plan[i], plan[i + 1], update, 0)

    fill(0)
    gather.settle()
    settle(r.columns.at[pl.ds(0, pairs - 1)], r.out_sem.at[0], place.partner)
    swaps_settle(("weights",))
    for step in second.relays():
        step()
    fill(1)

    def compute(chunk):
        a, b = 4 * chunk[0], 4 * (chunk[-1] + 1)
        number = (b - a) * count

        r.packed[0:number] = r.rows_two[a:b, :, 0:width].reshape(number, width)
        share = wide(r.rows_two[a:b, :, width:]).reshape(number, LANES)
        lane = lax.rem(lax.broadcasted_iota(jnp.int32, share.shape, 1), HALF)
        share = jnp.sum(jnp.where(lane == place.me // PIECES, share, 0.0), axis=1, keepdims=True)
        for i in range(2):
            for j in range(0, hidden_units, LANES):
                rows = r.packed[0:number]
                gated = clamped_unit(
                    jnp.dot(rows, r.wide_in[0, i, :, j : j + LANES], preferred_element_type=jnp.float32),
                    jnp.dot(rows, r.wide_in[1, i, :, j : j + LANES], preferred_element_type=jnp.float32),
                )
                at = i * hidden_units + j
                r.hidden[0:number, at : at + LANES] = gated.astype(jnp.bfloat16)
        for cut, lanes in enumerate(scatter.lanes):
            for j in range(lanes.start, lanes.start + lanes.size, LANES):
                weights = r.down[0, :, :, j : j + LANES].reshape(2 * hidden_units, LANES)
                units = r.hidden[0:number]
                part = jnp.dot(units, weights, preferred_element_type=jnp.float32)
                r.parts[a:b, :, j : j + LANES] = (
                    (part * share).astype(jnp.bfloat16).reshape(b - a, count, LANES)
                )
            for distance in reversed(chunk):
                scatter.first(distance, cut)

    for number, chunk in enumerate(chunks):
        second.across(number)
        if not number:
            for group in ("wide_in", "down"):
                loaded(group)
                swapped(group)
        compute(chunk)
    fill(2)
    second.settle()
    swaps_settle(("wide_in", "down"))
    for chunk in chunks:
        for cut in range(SUM_CUTS):
            for distance in reversed(chunk):
                scatter.last(distance, cut)
    fill(3)
    for cut in range(SUM_CUTS):
        scatter.collect(cut)
    moe = jnp.concatenate(scatter.values, axis=1)
    r.result[...] = (r.x_second[...] + rms_scale(moe) * r.gains[2]).astype(
        jnp.bfloat16
    )
    scatter.settle()


def store_kernel(result, new_state, result_hbm, state_hbm, sems):
    store = pltpu.make_async_copy(result, result_hbm, sems.at[0])
    store.start()
    for i in range(new_state.shape[0]):
        pltpu.make_async_copy(new_state.at[i], state_hbm.at[i], sems.at[1]).start()
    store.wait()
    pltpu.make_async_copy(new_state, state_hbm, sems.at[1]).wait()


def shards(
    residual_in,
    gain_mix_pre,
    w_query,
    w_key,
    w_value,
    w_outgate,
    w_decay,
    w_beta,
    decay_scale,
    decay_bias,
    head_gain,
    w_out,
    gain_mix_post,
    state_cache,
    gain_ffn_pre,
    routes,
    route_logits,
    w_gate,
    w_up,
    w_down,
    gain_ffn_post,
):
    devices = lax.axis_size("ep")
    layers, pairs = devices // 8, devices // 2
    count, width = residual_in.shape
    heads = w_decay.shape[1]
    own = w_query.shape[1]
    units = w_gate.shape[1]
    rows = 4 * max(1, layers // 2) * count
    if layers > 1:
        rows = max(rows, 4 * (layers - layers // 2) * count)
    inputs = dict(
        x=residual_in,
        gain=gain_mix_pre[None],
        routes=routes.T,
        logits=route_logits.T,
        w_decay=w_decay.T,
        w_beta=w_beta.T,
        scale=decay_scale[None],
        bias=decay_bias[None],
        head_gain=head_gain[None],
        gain_mix=gain_mix_post[None],
        gain_pre=gain_ffn_pre[None],
        gain_post=gain_ffn_post[None],
        query=w_query.T,
        key=w_key.T,
        value=w_value.T,
        outgate=w_outgate.T,
        state=state_cache,
        w_out=w_out,
        gate=w_gate,
        up=w_up,
        down=w_down,
    )
    bf16, f32 = jnp.bfloat16, jnp.float32
    dma = pltpu.SemaphoreType.DMA

    def blocks(number, lanes=width):
        return pltpu.VMEM((number, count, lanes), bf16)

    def per_head():
        return pltpu.VMEM((heads, count, HD), f32)

    def stacked(group):
        first = inputs[GROUPS[group][0]]
        pair = (2,) if group in PAIRED else ()
        many = (len(GROUPS[group]),) if group in PAIRED or len(GROUPS[group]) > 1 else ()
        return pltpu.VMEM(many + pair + first.shape, first.dtype)

    scratch = {group: stacked(group) for group in GROUPS}
    scratch |= dict(
        rows_one=blocks(pairs),
        rows_two=blocks(pairs, width + LANES),
        columns=blocks(pairs, 8 * own),
        joined=blocks(pairs, 8 * own),
        keys=per_head(),
        keep=per_head(),
        beta=per_head(),
        change=per_head(),
        x_second=pltpu.VMEM((count, width), f32),
        hidden=pltpu.VMEM((rows, 2 * units), bf16),
        packed=pltpu.VMEM((rows, width), bf16),
        parts=blocks(pairs),
        plane=blocks(3 * layers),
        column=blocks(layers),
        load_sems=dma((len(GROUPS),)),
        swap_send=dma((len(PAIRED),)),
        swap_recv=dma((len(PAIRED),)),
        one_send=dma((1,)),
        one_column=dma((layers,)),
        one_plane=dma((len(chunks_of(layers)),)),
        two_send=dma((1,)),
        two_column=dma((layers,)),
        two_plane=dma((len(chunks_of(layers)),)),
        out_sem=dma((1,)),
        in_sems=dma((layers,)),
        sum_send=dma((1,)),
        plane_recv=dma((layers, SUM_CUTS)),
        column_recv=dma((SUM_CUTS,)),
    )
    names = [name + "_hbm" for name in INPUTS] + ["result", "new_state"] + list(scratch)
    vmem = pl.BlockSpec(memory_space=pltpu.VMEM)
    hbm = pl.BlockSpec(memory_space=pltpu.HBM)
    held = pl.pallas_call(
        functools.partial(decode_kernel, devices, names),
        out_shape=(
            pltpu.VMEM((count, width), bf16),
            pltpu.VMEM(state_cache.shape, bf16),
        ),
        in_specs=[hbm] * len(INPUTS),
        out_specs=(vmem, vmem),
        scratch_shapes=list(scratch.values()),
        compiler_params=pltpu.CompilerParams(
            collective_id=0, has_side_effects=True, vmem_limit_bytes=VMEM_LIMIT
        ),
    )(*[inputs[name] for name in INPUTS])
    return pl.pallas_call(
        store_kernel,
        out_shape=[jax.ShapeDtypeStruct(a.shape, a.dtype) for a in held],
        in_specs=[vmem] * 2,
        out_specs=[hbm] * 2,
        scratch_shapes=[dma((2,))],
        compiler_params=pltpu.CompilerParams(vmem_limit_bytes=1000 * 1000),
    )(*held)


def solution(mesh):
    in_specs = (
        P("ep", None),
        P(),
        P(None, "ep"),
        P(None, "ep"),
        P(None, "ep"),
        P(None, "ep"),
        P(),
        P(),
        P(),
        P(),
        P(),
        P(),
        P(),
        P("ep", None, None, None),
        P(),
        P("ep", None),
        P("ep", None),
        P(None, "ep"),
        P(None, "ep"),
        P("ep", None),
        P(),
    )
    out_specs = (P("ep", None), P("ep", None, None, None))
    return jax.shard_map(shards, mesh=mesh, in_specs=in_specs, out_specs=out_specs, check_vma=False)
```

time: 45.3 us -> 43.6 us (0.962)
  Pallas kernels: 44.5 us -> 42.8 us
    pallas_call x1, Pallas kernels: 42.4 us -> 40.8 us  [shards(): pl.pallas_call(functools.partial(decode_kernel, devices, names), out_shap...]
where the time goes in v2:
time: 43.6 us; the launch traced here: 43.5 us
  Pallas kernels  42.8 us (98%)
  between operations  0.65 us (1%)
    pallas_call x1, Pallas kernels, shards(): pl.pallas_call(functools.partial(decode_kernel, devices, names), out_shap...  40.8 us
    pallas_call x1, Pallas kernels, shards(): pl.pallas_call(store_kernel, out_shape=[jax.ShapeDtypeStruct(a.shape, a.d...  2.03 us

profile of v2, /device:TPU:0, one launch (start us, length us, event | category | flops | bytes accessed | tf_op | source)
XLA Modules:
  0.0 43.5 jit_solution(2087225845104043834)
XLA Ops:
  0.6 40.8 %shard_map.212 = (bf16[8,2048]{1,0:T(8,128)(2,1)S(1)}, bf16[8,16,128,128]{3,2,1,0:T(8,128)(2,1)S(1)}) custom-call(bf16[8,2048]{1,0:T(8,128)(2,1)} %refs_0_.1, f32[1,2048]{1,0:T(1,128)} %bitcast.21, s32[4,8]{1,0:T(4,128)} %bitcast.25, f32[4,8]{1,0:T(4,128)} %bitcast.26, bf16[16,2048]{1,0:T(8,128)(2,1)} %bitcast.19, bf16[16,2048]{1,0:T(8,128)(2,1)} %bitcast.20, ...), custom_call_target="tpu_custom_call" | custom-call | tf_op jit(solution)/shard_map/pallas_call | solution.py:644
  41.4 2.0 %shard_map.213 = (bf16[8,2048]{1,0:T(8,128)(2,1)}, bf16[8,16,128,128]{3,2,1,0:T(8,128)(2,1)}) custom-call(bf16[8,2048]{1,0:T(8,128)(2,1)S(1)} %get-tuple-element.4.result, bf16[8,16,128,128]{3,2,1,0:T(8,128)(2,1)S(1)} %get-tuple-element.5.new_state), custom_call_target="tpu_custom_call" | custom-call | tf_op jit(solution)/shard_map/pallas_call | solution.py:657

commit v3 on v2

--- a/solution.py
+++ b/solution.py
@@ -357,15 +357,18 @@
     load(LATE)
     for step in gather.relays():
         step()
+    loaded("weights")
+    swapped("weights")
+    for j in range(0, width, 256):
+        r.upright[j : j + 256] = jnp.transpose(
+            r.weights[:, :, :, j : j + 256].reshape(4 * piece, 256)
+        )
     for number, chunk in enumerate(chunks):
         gather.across(number)
-        if not number:
-            loaded("weights")
-            swapped("weights")
         a, b = 4 * chunk[0], 4 * (chunk[-1] + 1)
         rows = r.rows_one[a:b].reshape((b - a) * count, width)
-        weights = r.weights[...].reshape(4 * piece, width)
-        r.columns[a:b] = dot_t(rows, weights).astype(jnp.bfloat16).reshape(b - a, count, 4 * piece)
+        product = jnp.dot(rows, r.upright[...], preferred_element_type=jnp.float32)
+        r.columns[a:b] = product.astype(jnp.bfloat16).reshape(b - a, count, 4 * piece)
         for distance in reversed(chunk):
             for y, x in ((1, 1), (0, 1), (1, 0), (0, 0)):
                 if (distance, y, x) == (0, 0, 0):
@@ -442,8 +445,6 @@
         jnp.bfloat16
     )
     second = Gather(place, r.rows_two, r.two_send, r.two_column, r.two_plane)
-    second.begin()
-
     def update(h, carry):
         upright = jnp.transpose(r.keys[h])
         change, keep = r.change[h], r.keep[h]
@@ -468,7 +469,10 @@
     def fill(i):
         lax.fori_loop(plan[i], plan[i + 1], update, 0)
 
-    fill(0)
+    ahead = core * (heads * 3 // 16)
+    lax.fori_loop(0, ahead, update, 0)
+    second.begin()
+    lax.fori_loop(ahead, plan[1], update, 0)
     gather.settle()
     settle(r.columns.at[pl.ds(0, pairs - 1)], r.out_sem.at[0], place.partner)
     swaps_settle(("weights",))
@@ -485,21 +489,21 @@
         lane = lax.rem(lax.broadcasted_iota(jnp.int32, share.shape, 1), HALF)
         share = jnp.sum(jnp.where(lane == place.me // PIECES, share, 0.0), axis=1, keepdims=True)
         for i in range(2):
-            for j in range(0, hidden_units, LANES):
+            for j in range(0, hidden_units, 128):
                 rows = r.packed[0:number]
                 gated = clamped_unit(
-                    jnp.dot(rows, r.wide_in[0, i, :, j : j + LANES], preferred_element_type=jnp.float32),
-                    jnp.dot(rows, r.wide_in[1, i, :, j : j + LANES], preferred_element_type=jnp.float32),
+                    jnp.dot(rows, r.wide_in[0, i, :, j : j + 128], preferred_element_type=jnp.float32),
+                    jnp.dot(rows, r.wide_in[1, i, :, j : j + 128], preferred_element_type=jnp.float32),
                 )
                 at = i * hidden_units + j
-                r.hidden[0:number, at : at + LANES] = gated.astype(jnp.bfloat16)
+                r.hidden[0:number, at : at + 128] = gated.astype(jnp.bfloat16)
         for cut, lanes in enumerate(scatter.lanes):
-            for j in range(lanes.start, lanes.start + lanes.size, LANES):
-                weights = r.down[0, :, :, j : j + LANES].reshape(2 * hidden_units, LANES)
+            for j in range(lanes.start, lanes.start + lanes.size, 512):
+                weights = r.down[0, :, :, j : j + 512].reshape(2 * hidden_units, 512)
                 units = r.hidden[0:number]
                 part = jnp.dot(units, weights, preferred_element_type=jnp.float32)
-                r.parts[a:b, :, j : j + LANES] = (
-                    (part * share).astype(jnp.bfloat16).reshape(b - a, count, LANES)
+                r.parts[a:b, :, j : j + 512] = (
+                    (part * share).astype(jnp.bfloat16).reshape(b - a, count, 512)
                 )
             for distance in reversed(chunk):
                 scatter.first(distance, cut)
@@ -609,6 +613,7 @@
 
     scratch = {group: stacked(group) for group in GROUPS}
     scratch |= dict(
+        upright=pltpu.VMEM((width, 8 * own), bf16),
         rows_one=blocks(pairs),
         rows_two=blocks(pairs, width + LANES),
         columns=blocks(pairs, 8 * own),

time: 43.6 us -> 42.9 us (0.984)
  Pallas kernels: 42.8 us -> 42.1 us
    pallas_call x1, Pallas kernels: 40.8 us -> 40.1 us  [shards(): pl.pallas_call(functools.partial(decode_kernel, devices, names), out_shap...]
where the time goes in v3:
time: 42.9 us; the launch traced here: 42.8 us
  Pallas kernels  42.1 us (98%)
  between operations  0.65 us (2%)
    pallas_call x1, Pallas kernels, shards(): pl.pallas_call(functools.partial(decode_kernel, devices, names), out_shap...  40.1 us
    pallas_call x1, Pallas kernels, shards(): pl.pallas_call(store_kernel, out_shape=[jax.ShapeDtypeStruct(a.shape, a.d...  2.03 us

profile of v3, /device:TPU:0, one launch (start us, length us, event | category | flops | bytes accessed | tf_op | source)
XLA Modules:
  0.0 42.8 jit_solution(7246729842256651855)
XLA Ops:
  0.6 40.1 %shard_map.212 = (bf16[8,2048]{1,0:T(8,128)(2,1)S(1)}, bf16[8,16,128,128]{3,2,1,0:T(8,128)(2,1)S(1)}) custom-call(bf16[8,2048]{1,0:T(8,128)(2,1)} %refs_0_.1, f32[1,2048]{1,0:T(1,128)} %bitcast.21, s32[4,8]{1,0:T(4,128)} %bitcast.25, f32[4,8]{1,0:T(4,128)} %bitcast.26, bf16[16,2048]{1,0:T(8,128)(2,1)} %bitcast.19, bf16[16,2048]{1,0:T(8,128)(2,1)} %bitcast.20, ...), custom_call_target="tpu_custom_call" | custom-call | tf_op jit(solution)/shard_map/pallas_call | solution.py:649
  40.7 2.0 %shard_map.213 = (bf16[8,2048]{1,0:T(8,128)(2,1)}, bf16[8,16,128,128]{3,2,1,0:T(8,128)(2,1)}) custom-call(bf16[8,2048]{1,0:T(8,128)(2,1)S(1)} %get-tuple-element.4.result, bf16[8,16,128,128]{3,2,1,0:T(8,128)(2,1)S(1)} %get-tuple-element.5.new_state), custom_call_target="tpu_custom_call" | custom-call | tf_op jit(solution)/shard_map/pallas_call | solution.py:662
